TPU v7x, 32 devices: a whole 2x2x4 slice. The times are simulated.
32 devices in a mesh: sp: 4 (over z), fs: 4 (over y, x), tp: 2 (over core).
Axes of the slice: x: 2, y: 2, z: 4, core: 2. Of those that a mesh axis runs over, the one named last changes fastest.
Arguments:
- tokens: bfloat16 [4, 640, 2048], P('fs', 'sp', 'tp'), may hold values from -6 to 6
- mix_gain: float32 [2048], replicated, may hold values from 0.1 to 1.9
- conv_b_weight: bfloat16 [2048, 1024], P(('sp', 'fs'), 'tp'), may hold values from -0.125 to 0.125
- conv_c_weight: bfloat16 [2048, 1024], P(('sp', 'fs'), 'tp'), may hold values from -0.125 to 0.125
- conv_v_weight: bfloat16 [2048, 1024], P(('sp', 'fs'), 'tp'), may hold values from -0.125 to 0.125
- conv_taps: float32 [3, 1024], P(None, 'tp'), may hold values from -3.5 to 3.5
- query_weight: bfloat16 [2048, 2048], P(('sp', 'fs'), 'tp'), may hold values from -0.125 to 0.125
- query_rope_weight: bfloat16 [2048, 1024], P(('sp', 'fs'), 'tp'), may hold values from -4.5 to 4.5
- latent_weight: bfloat16 [2048, 512], P(('sp', 'fs')), may hold values from -0.125 to 0.125
- key_rope_weight: bfloat16 [2048, 64], replicated, may hold values from -1 to 1
- latent_gain: float32 [512], replicated, may hold values from 0.1 to 1.9
- key_up_weight: bfloat16 [512, 2048], P(None, 'tp'), may hold values from -0.25 to 0.25
- value_up_weight: bfloat16 [512, 2048], P(None, 'tp'), may hold values from -0.25 to 0.25
- head_gain: float32 [2048], P('tp'), may hold values from 0.1 to 1.9
- conv_out_weight: bfloat16 [1024, 2048], P('tp', ('sp', 'fs')), may hold values from -0.109375 to 0.109375
- attn_out_weight: bfloat16 [2048, 2048], P('tp', ('sp', 'fs')), may hold values from -0.109375 to 0.109375
Outputs:
- mixed: bfloat16 [4, 640, 2048], P('fs', ('sp', 'tp'))
All inputs are finite; a program needn't handle non-finite values.
Results may differ from a plain program's by a relative error of at most 0.025.
Values may be sent and summed in bfloat16 or wider, within the bound.
No kernel may reach another device: no remote copies, remote signals or barrier semaphores. Data moves between devices by JAX's collectives and lax.ppermute only.
A program may use at most 128 MiB of HBM per device.

v0:
```python
import jax
import jax.numpy as jnp
from jax import lax
from jax.sharding import PartitionSpec as P

NOPE = 128
ROPE = 64
VD = 128
KVL = 512
SEG = 64
norm_epsilon = 1e-06
rope_theta = 10000.0


def passed_along(block, axis, distance):
    devices = range(lax.axis_size(axis))
    route = [(i - distance, i) for i in devices if i - distance in devices]
    return lax.ppermute(block, axis, route)


def rms_scale(values, gain):
    return (
        values * lax.rsqrt(jnp.mean(values * values, axis=-1, keepdims=True) + norm_epsilon) * gain
    )


def rope_tables(positions):
    half_width = ROPE // 2
    frequency = rope_theta ** (-jnp.arange(half_width, dtype=jnp.float32) * 2.0 / ROPE)
    angles = positions[:, None] * frequency[None, :]
    return (jnp.cos(angles), jnp.sin(angles))


def rotate(values, cosine, sine):
    half_width = ROPE // 2
    first = values[..., :half_width]
    second = values[..., half_width:]
    return jnp.concatenate(
        [first * cosine - second * sine, second * cosine + first * sine], axis=-1
    )


def shards(
    tokens,
    mix_gain,
    conv_b_weight,
    conv_c_weight,
    conv_v_weight,
    conv_taps,
    query_weight,
    query_rope_weight,
    latent_weight,
    key_rope_weight,
    latent_gain,
    key_up_weight,
    value_up_weight,
    head_gain,
    conv_out_weight,
    attn_out_weight,
):
    full_rows = lax.all_gather(tokens[0], "tp", axis=1, tiled=True)
    tok_rows = full_rows.shape[0]
    normed = rms_scale(full_rows.astype(jnp.float32), mix_gain).astype(jnp.bfloat16)
    offset = lax.axis_index("sp") * tok_rows
    token_index = offset + jnp.arange(tok_rows, dtype=jnp.int32)
    cosine, sine = rope_tables(token_index.astype(jnp.float32))
    local_heads = query_weight.shape[1] // NOPE
    count_sp = lax.axis_size("sp")
    count_fs = lax.axis_size("fs")
    count_tp = lax.axis_size("tp")
    fs_index = lax.axis_index("fs")
    row_piece = normed.shape[1] // (count_sp * count_fs)
    all_normed = lax.all_gather(normed, "fs", axis=0, tiled=True)
    picked = lax.dynamic_index_in_dim(
        all_normed.reshape(-1, count_sp, count_fs, row_piece), fs_index, 2, keepdims=False
    ).reshape(-1, count_sp * row_piece)
    gathered = (
        lax.all_gather(conv_b_weight, "sp", axis=0, tiled=True),
        lax.all_gather(conv_c_weight, "sp", axis=0, tiled=True),
        lax.all_gather(conv_v_weight, "sp", axis=0, tiled=True),
        lax.all_gather(query_weight, "sp", axis=0, tiled=True),
        lax.all_gather(query_rope_weight, "sp", axis=0, tiled=True),
        lax.all_gather(latent_weight, "sp", axis=0, tiled=True),
    )

    def project_in():
        return jnp.concatenate(
            [jnp.dot(picked, member, preferred_element_type=jnp.float32) for member in gathered],
            axis=1,
        )

    joined = lax.psum_scatter(
        project_in().astype(jnp.bfloat16), "fs", scatter_dimension=0, tiled=True
    ).astype(jnp.float32)
    bounds = []
    running_total = 0
    for member in gathered[:-1]:
        running_total = running_total + member.shape[1]
        bounds.append(running_total)
    sums = tuple(jnp.split(joined, bounds, axis=1))
    latent_raw = sums[5].astype(jnp.bfloat16)
    gate_b = sums[0].astype(jnp.bfloat16)
    gate_c = sums[1].astype(jnp.bfloat16)
    values_v = sums[2].astype(jnp.bfloat16)
    query_nope = sums[3].astype(jnp.bfloat16).reshape(tok_rows, local_heads, NOPE)
    query_rot = rotate(
        sums[4].reshape(tok_rows, local_heads, ROPE), cosine[:, None, :], sine[:, None, :]
    ).astype(jnp.bfloat16)
    latent = rms_scale(latent_raw.astype(jnp.float32), latent_gain).astype(jnp.bfloat16)
    key_rot = rotate(
        jnp.dot(normed, key_rope_weight, preferred_element_type=jnp.float32), cosine, sine
    ).astype(jnp.bfloat16)
    query_latent = jnp.einsum(
        "thn,khn->thk",
        query_nope,
        key_up_weight.reshape(KVL, local_heads, NOPE),
        preferred_element_type=jnp.float32,
    ).astype(jnp.bfloat16)
    attn_scale = (NOPE + ROPE) ** (-0.5)
    product = (gate_c.astype(jnp.float32) * values_v.astype(jnp.float32)).astype(jnp.bfloat16)
    previous = passed_along(product[tok_rows - 2 :], "sp", 1)
    padded = jnp.concatenate([previous, product], axis=0).astype(jnp.float32)
    convolved = (
        conv_taps[0] * padded[0:tok_rows]
        + conv_taps[1] * padded[1 : tok_rows + 1]
        + conv_taps[2] * padded[2 : tok_rows + 2]
    )
    conv_y = (gate_b.astype(jnp.float32) * convolved).astype(jnp.bfloat16)
    query_segment = token_index // SEG
    last_segment = (offset + tok_rows - 1) // SEG

    def key_block(running, latent_block, rot_block, first_key):
        peak_old, denom_old, accum_old = running
        block_rows = latent_block.shape[0]
        scores = (
            jnp.einsum(
                "thk,jk->thj", query_latent, latent_block, preferred_element_type=jnp.float32
            )
            + jnp.einsum("thr,jr->thj", query_rot, rot_block, preferred_element_type=jnp.float32)
        ) * attn_scale
        key_segment = (first_key + jnp.arange(block_rows, dtype=jnp.int32)) // SEG
        allowed = key_segment[None, None, :] <= query_segment[:, None, None]
        peak_new = jnp.maximum(peak_old, jnp.max(jnp.where(allowed, scores, -1e30), axis=-1))
        weights = jnp.where(allowed, jnp.exp(scores - peak_new[..., None]), 0.0)
        rescale = jnp.exp(peak_old - peak_new)
        denom_new = denom_old * rescale + jnp.sum(weights, axis=-1)
        accum_new = accum_old * rescale[..., None] + jnp.einsum(
            "thj,jk->thk",
            weights.astype(jnp.bfloat16),
            latent_block,
            preferred_element_type=jnp.float32,
        )
        return (peak_new, denom_new, accum_new)

    starting = (
        jnp.full((tok_rows, local_heads), -1e30, jnp.float32),
        jnp.zeros((tok_rows, local_heads), jnp.float32),
        jnp.zeros((tok_rows, local_heads, KVL), jnp.float32),
    )
    latent_piece = lax.all_gather(latent, "sp", axis=0, tiled=True)
    rot_piece = lax.all_gather(key_rot, "sp", axis=0, tiled=True)
    piece_rows = latent_piece.shape[0]
    splits = max(1, piece_rows // 512)
    while piece_rows % splits:
        splits = splits - 1
    block_rows = piece_rows // splits

    def visit(state, block_index):
        block_begin = block_index * block_rows
        latent_block = lax.dynamic_slice_in_dim(latent_piece, block_begin, block_rows, 0)
        rot_block = lax.dynamic_slice_in_dim(rot_piece, block_begin, block_rows, 0)
        updated = lax.cond(
            block_begin // SEG <= last_segment,
            lambda inner: key_block(inner, latent_block, rot_block, block_begin),
            lambda inner: inner,
            state,
        )
        return (updated, None)

    peak, denom, accum = lax.scan(visit, starting, jnp.arange(splits, dtype=jnp.int32))[0]
    attended = (accum / denom[..., None]).astype(jnp.bfloat16)
    head_out = jnp.einsum(
        "thk,khv->thv",
        attended,
        value_up_weight.reshape(KVL, local_heads, VD),
        preferred_element_type=jnp.float32,
    )
    normed_heads = rms_scale(head_out, head_gain.reshape(local_heads, VD))
    attn_y = normed_heads.astype(jnp.bfloat16).reshape(tok_rows, local_heads * VD)
    share_rows = tok_rows // count_tp
    conv_all, attn_all = (
        lax.all_gather(conv_y, "fs", axis=0, tiled=True),
        lax.all_gather(attn_y, "fs", axis=0, tiled=True),
    )
    conv_sorted = (
        conv_all.reshape(count_fs, count_tp, share_rows, -1)
        .transpose(1, 0, 2, 3)
        .reshape(count_fs * tok_rows, -1)
    )
    attn_sorted = (
        attn_all.reshape(count_fs, count_tp, share_rows, -1)
        .transpose(1, 0, 2, 3)
        .reshape(count_fs * tok_rows, -1)
    )
    conv_cols_sp, attn_cols_sp = (
        lax.all_gather(conv_out_weight, "sp", axis=1, tiled=True),
        lax.all_gather(attn_out_weight, "sp", axis=1, tiled=True),
    )
    col_sums = lax.psum_scatter(
        (
            jnp.dot(conv_sorted, conv_cols_sp, preferred_element_type=jnp.float32)
            + jnp.dot(attn_sorted, attn_cols_sp, preferred_element_type=jnp.float32)
        ).astype(jnp.bfloat16),
        "tp",
        scatter_dimension=0,
        tiled=True,
    )
    col_piece = conv_cols_sp.shape[1] // count_sp
    outgoing = col_sums.reshape(count_fs, share_rows, count_sp * col_piece)
    arrived = lax.all_to_all(outgoing, "fs", split_axis=0, concat_axis=2, tiled=True)
    result = (
        arrived.reshape(share_rows, count_fs, count_sp, col_piece)
        .transpose(0, 2, 1, 3)
        .reshape(share_rows, count_fs * count_sp * col_piece)
    )
    return result[None]


def solution(mesh):
    return jax.shard_map(
        shards,
        mesh=mesh,
        in_specs=(
            P("fs", "sp", "tp"),
            P(),
            P(("sp", "fs"), "tp"),
            P(("sp", "fs"), "tp"),
            P(("sp", "fs"), "tp"),
            P(None, "tp"),
            P(("sp", "fs"), "tp"),
            P(("sp", "fs"), "tp"),
            P(("sp", "fs"), None),
            P(),
            P(),
            P(None, "tp"),
            P(None, "tp"),
            P("tp"),
            P("tp", ("sp", "fs")),
            P("tp", ("sp", "fs")),
        ),
        out_specs=P("fs", ("sp", "tp"), None),
        check_vma=False,
    )
```

profile of v0, /device:TPU:0, one launch (start us, length us, event | category | flops | bytes accessed | tf_op | source)
XLA Modules:
  0.0 311.9 jit_solution(16413146177102707444)
XLA Ops:
  6.6 2.7 all-gather
  9.5 1.8 fusion.22
  12.2 17.5 %all_gather.44 = bf16[512,512]{1,0:T(8,128)(2,1)S(1)} all-gather(bf16[128,512]{1,0:T(8,128)(2,1)S(1)} %copy-done.9), channel_id=1, replica_groups=mesh['sp'=4,'fs'=4,'tp'=2] {'sp'}, dimensions={0}, use_global_device_ids=true | all-gather | bytes 655360 | tf_op jit(solution)/shard_map/all_gather | solution.py:78
  29.6 16.5 %all_gather.45 = bf16[512,512]{1,0:T(8,128)(2,1)} all-gather(bf16[128,512]{1,0:T(8,128)(2,1)S(1)} %copy-done.10), channel_id=1, replica_groups=mesh['sp'=4,'fs'=4,'tp'=2] {'sp'}, dimensions={0}, use_global_device_ids=true | all-gather | bytes 655360 | tf_op jit(solution)/shard_map/all_gather | solution.py:79
  46.1 16.7 %all_gather.46 = bf16[512,512]{1,0:T(8,128)(2,1)} all-gather(bf16[128,512]{1,0:T(8,128)(2,1)S(1)} %copy-done.11), channel_id=1, replica_groups=mesh['sp'=4,'fs'=4,'tp'=2] {'sp'}, dimensions={0}, use_global_device_ids=true | all-gather | bytes 655360 | tf_op jit(solution)/shard_map/all_gather | solution.py:80
  62.8 22.8 %all_gather.48 = bf16[512,512]{1,0:T(8,128)(2,1)S(1)} all-gather(bf16[128,512]{1,0:T(8,128)(2,1)S(1)} %copy-done.12), channel_id=1, replica_groups=mesh['sp'=4,'fs'=4,'tp'=2] {'sp'}, dimensions={0}, use_global_device_ids=true | all-gather | bytes 655360 | tf_op jit(solution)/shard_map/all_gather | solution.py:82
  85.6 17.8 %all_gather.49 = bf16[512,512]{1,0:T(8,128)(2,1)} all-gather(bf16[128,512]{1,0:T(8,128)(2,1)S(1)} %copy-done.13), channel_id=1, replica_groups=mesh['sp'=4,'fs'=4,'tp'=2] {'sp'}, dimensions={0}, use_global_device_ids=true | all-gather | bytes 655360 | tf_op jit(solution)/shard_map/all_gather | solution.py:83
  103.4 4.4 %copy.65 = bf16[640,2048]{0,1:T(8,128)(2,1)} copy(bf16[640,2048]{1,0:T(8,128)(2,1)} %all-gather.7.cloned.1.call-done) | data formatting | bytes 5242880 | tf_op jit(solution)/shard_map/all_gather | solution.py:73
  107.8 1.1 constant_dynamic-slice_fusion
  109.9 2.5 convolution_convert_fusion.5
  112.4 1.3 copy.69
  113.8 2.5 convolution_convert_fusion.4
  116.3 1.3 copy.70
  117.6 0.9 constant_dynamic-update-slice_fusion.2
  119.4 0.9 constant_dynamic-update-slice_fusion
  120.4 3.3 %fusion.15 = bf16[640,3584]{1,0:T(8,128)(2,1)} fusion(bf16[640,3584]{1,0:T(8,128)(2,1)} %constant_dynamic-update-slice_fusion, bf16[640,512]{0,1:T(8,128)(2,1)S(1)} %bitcast.104, bf16[512,1024]{1,0:T(8,128)(2,1)} %all-gather.9.cloned.1.call-done), kind=kOutput, calls=%fused_computation.35 | convolution fusion | flops 671744000 | bytes 3014656 | tf_op jit(solution)/shard_map/dot_general | solution.py:88
  123.6 1.4 fusion.19
  125.0 1.4 fusion.18
  126.6 1.0 copy-done.3
  128.4 1.9 broadcast_in_dim.56
  130.3 14.1 %all-gather.1 = bf16[4,160,64]{1,2,0:T(8,128)(2,1)} all-gather(bf16[1,160,64]{1,2,0:T(8,128)(2,1)S(1)} %maximum_bitcast_fusion), channel_id=1, replica_groups=mesh['sp'=4,'fs'=4,'tp'=2] {'sp'}, dimensions={0}, use_global_device_ids=true | all-gather | bytes 102400 | tf_op jit(solution)/shard_map/all_gather | solution.py:161
  144.3 36.4 %reduce-scatter.3.cloned.1.call-done = bf16[160,3584]{1,0:T(8,128)(2,1)} async-done(((bf16[640,3584]{1,0:T(8,128)(2,1)}), bf16[160,3584]{1,0:T(8,128)(2,1)}) %reduce-scatter.3.cloned.1.call-update) | async-done | bytes 1146896 | tf_op jit(solution)/shard_map/reduce_scatter | solution.py:92
  180.7 1.0 fusion.32
  181.8 1.8 fusion.34
  183.6 17.8 %all_gather.52 = bf16[640,512]{1,0:T(8,128)(2,1)S(1)} all-gather(bf16[160,512]{1,0:T(8,128)(2,1)S(1)} %get-tuple-element.251), channel_id=1, replica_groups=mesh['sp'=4,'fs'=4,'tp'=2] {'sp'}, dimensions={0}, use_global_device_ids=true | all-gather | bytes 819200 | tf_op jit(solution)/shard_map/all_gather | solution.py:160
  201.4 0.9 slice_convert_fusion
  203.0 1.5 fusion.16
  204.5 12.2 %conditional.1 = ((f32[160,8]{1,0:T(8,128)S(1)}, f32[160,8,512]{2,1,0:T(8,128)})) conditional(s32[]{:T(128)} %convert_element_type.79, (f32[160,8]{1,0:T(8,128)S(1)}, f32[160,8,512]{2,1,0:T(8,128)}) %tuple.31, (s32[160]{0:T(256)S(1)}, s32[160]{0:T(256)S(1)}, s32[]{:T(128)}, bf16[160,8,512]{2,0,1:T(8,128)(2,1)S(1)}, ...), branch_computations={%region_3.4_spmd, %region_4.7_spmd.clone} | conditional | flops 1792195712 | bytes 46272084 | solution.py:172
  204.9 1.7 copy.85
  206.5 1.7 reshape.204
  208.2 1.5 fusion.9
  209.7 1.9 select_reduce_fusion
  211.6 1.1 fusion.1
  213.3 1.8 multiply_add_fusion
  215.1 1.5 copy-done.2
  216.7 2.1 divide_convert_fusion
  218.8 1.1 multiply_reduce_fusion
  219.9 1.0 copy_bitcast_fusion
  221.6 2.5 collective-permute-start
  224.1 15.4 %all_gather.51 = bf16[512,512]{1,0:T(8,128)(2,1)S(1)} all-gather(bf16[512,128]{1,0:T(8,128)(2,1)S(1)} %copy-done.14), channel_id=1, replica_groups=mesh['sp'=4,'fs'=4,'tp'=2] {'sp'}, dimensions={1}, use_global_device_ids=true | all-gather | bytes 655360 | tf_op jit(solution)/shard_map/all_gather | solution.py:206
  239.5 1.0 fusion.40
  240.6 12.5 %all_gather.50 = bf16[640,512]{1,0:T(8,128)(2,1)S(1)} all-gather(bf16[160,512]{1,0:T(8,128)(2,1)S(1)} %fusion.40), channel_id=1, replica_groups=mesh['sp'=4,'fs'=4,'tp'=2] {'fs'}, dimensions={0}, use_global_device_ids=true | all-gather | bytes 819200 | tf_op jit(solution)/shard_map/all_gather | solution.py:192
  253.6 2.5 copy.81
  256.1 26.6 %all-gather.13.cloned.1.call-done = bf16[1024,512]{1,0:T(8,128)(2,1)} async-done(((bf16[1024,128]{1,0:T(8,128)(2,1)}), bf16[1024,512]{1,0:T(8,128)(2,1)}) %all-gather.13.cloned.1.call-update) | async-done | bytes 1048592 | tf_op jit(solution)/shard_map/all_gather | solution.py:207
  282.8 3.3 %fusion.17 = bf16[640,512]{1,0:T(8,128)(2,1)} fusion(f32[640,512]{1,0:T(8,128)S(1)} %fusion.44, bf16[640,1024]{1,0:T(8,128)(2,1)} %bitcast.98, bf16[1024,512]{1,0:T(8,128)(2,1)} %all-gather.13.cloned.1.call-done), kind=kOutput, calls=%fused_computation.38 | convolution fusion | flops 671744000 | bytes 4325376 | tf_op jit(solution)/shard_map/dot_general | solution.py:212
  286.1 6.5 %reduce-scatter.5.cloned.1.call-done = bf16[320,512]{1,0:T(8,128)(2,1)} async-done(((bf16[640,512]{1,0:T(8,128)(2,1)}), bf16[320,512]{1,0:T(8,128)(2,1)}) %reduce-scatter.5.cloned.1.call-update) | async-done | bytes 327696 | tf_op jit(solution)/shard_map/reduce_scatter | solution.py:209
  292.6 11.0 %all_to_all.15 = bf16[4,80,512]{2,1,0:T(8,128)(2,1)S(1)} all-to-all(bf16[4,80,512]{2,1,0:T(8,128)(2,1)} %bitcast.107), channel_id=1, replica_groups=mesh['sp'=4,'fs'=4,'tp'=2] {'fs'}, dimensions={0} | all-to-all | bytes 655360 | tf_op jit(solution)/shard_map/all_to_all | solution.py:220
  304.1 1.0 broadcast_in_dim_reshape.4
  (83 shorter events, 7.0 us)
Async XLA Ops:
  6.5 196.5 %copy-start = (bf16[512,1024]{1,0:T(8,128)(2,1)S(1)}, bf16[512,1024]{1,0:T(8,128)(2,1)}, u32[]{:S(2)}) copy-start(bf16[512,1024]{1,0:T(8,128)(2,1)} %param.29) | copy-start | bytes 3145732
  6.5 5.6 %copy-start.9 = (bf16[128,512]{1,0:T(8,128)(2,1)S(1)}, bf16[128,512]{1,0:T(8,128)(2,1)}, u32[]{:S(2)}) copy-start(bf16[128,512]{1,0:T(8,128)(2,1)} %param.20) | copy-start | bytes 393220
  6.5 23.1 %copy-start.10 = (bf16[128,512]{1,0:T(8,128)(2,1)S(1)}, bf16[128,512]{1,0:T(8,128)(2,1)}, u32[]{:S(2)}) copy-start(bf16[128,512]{1,0:T(8,128)(2,1)} %param.21) | copy-start | bytes 393220
  6.5 39.6 %copy-start.11 = (bf16[128,512]{1,0:T(8,128)(2,1)S(1)}, bf16[128,512]{1,0:T(8,128)(2,1)}, u32[]{:S(2)}) copy-start(bf16[128,512]{1,0:T(8,128)(2,1)} %param.22) | copy-start | bytes 393220
  6.5 96.9 %all-gather.7.cloned.1.call-start = ((), (), s32[]{:S(2)}) async-start(), calls=%async_computation.3 | async-start | bytes 3276800 | tf_op jit(solution)/shard_map/all_gather | solution.py:73
  9.3 53.5 %copy-start.12 = (bf16[128,512]{1,0:T(8,128)(2,1)S(1)}, bf16[128,512]{1,0:T(8,128)(2,1)}, u32[]{:S(2)}) copy-start(bf16[128,512]{1,0:T(8,128)(2,1)} %param.25) | copy-start | bytes 393220
  9.3 76.3 %copy-start.13 = (bf16[128,512]{1,0:T(8,128)(2,1)S(1)}, bf16[128,512]{1,0:T(8,128)(2,1)}, u32[]{:S(2)}) copy-start(bf16[128,512]{1,0:T(8,128)(2,1)} %param.26) | copy-start | bytes 393220
  11.4 109.0 %all-gather.9.cloned.1.call-start = ((), (), s32[]{:S(2)}) async-start(), calls=%async_computation.4 | async-start | bytes 1310720 | tf_op jit(solution)/shard_map/all_gather | solution.py:81
  12.1 168.6 %reduce-scatter.3.cloned.1.call-start = ((), (), s32[]{:S(2)}) async-start(), calls=%async_computation.5 | async-start | bytes 5734400 | tf_op jit(solution)/shard_map/reduce_scatter | solution.py:92
  109.0 4.8 %copy-start.5 = (bf16[640,4,1,128]{0,3,2,1:T(8,128)(2,1)}, bf16[640,4,1,128]{0,3,2,1:T(8,128)(2,1)S(1)}, u32[]{:S(2)}) copy-start(bf16[640,4,1,128]{0,3,2,1:T(8,128)(2,1)S(1)} %constant_dynamic-slice_fusion) | copy-start | bytes 1966084
  118.5 1.8 copy-start.6
  120.4 4.7 %copy-start.7 = (bf16[512,512]{1,0:T(8,128)(2,1)S(1)}, bf16[512,512]{1,0:T(8,128)(2,1)}, u32[]{:S(2)}) copy-start(bf16[512,512]{1,0:T(8,128)(2,1)} %all_gather.49) | copy-start | bytes 1572868
  126.5 1.1 copy-start.3
  126.5 1.1 copy-start.8
  126.5 55.3 %copy-start.17 = (f32[512]{0:T(512)S(1)}, f32[512]{0:T(512)}, u32[]{:S(2)}) copy-start(f32[512]{0:T(512)} %param.28) | copy-start | bytes 6148
  126.5 127.1 %all-gather.11.cloned.1.call-start = ((), (), s32[]{:S(2)}) async-start(), calls=%async_computation.6 | async-start | bytes 1638400 | tf_op jit(solution)/shard_map/all_gather | solution.py:193
  211.6 1.7 copy-start.1
  215.1 1.5 copy-start.2
  216.7 2.1 copy-start.18
  218.8 1.1 copy-start.16
  218.8 2.8 copy-start.15
  218.8 2.8 copy-start.4
  218.8 5.3 %copy-start.14 = (bf16[512,128]{1,0:T(8,128)(2,1)S(1)}, bf16[512,128]{1,0:T(8,128)(2,1)}, u32[]{:S(2)}) copy-start(bf16[512,128]{1,0:T(8,128)(2,1)} %param.32) | copy-start | bytes 393220
  220.9 61.9 %all-gather.13.cloned.1.call-start = ((), (), s32[]{:S(2)}) async-start(), calls=%async_computation.7 | async-start | bytes 1310720 | tf_op jit(solution)/shard_map/all_gather | solution.py:207
  221.5 71.1 %reduce-scatter.5.cloned.1.call-start = ((), (), s32[]{:S(2)}) async-start(), calls=%async_computation.8 | async-start | bytes 983040 | tf_op jit(solution)/shard_map/reduce_scatter | solution.py:209
  221.6 17.9 %collective-permute-start = (bf16[2,512]{1,0:T(2,128)(2,1)S(1)}, bf16[2,512]{1,0:T(2,128)(2,1)S(1)}, u32[]{:S(2)}, u32[]{:S(2)}) collective-permute-start(bf16[2,512]{1,0:T(2,128)(2,1)S(1)} %slice.44), channel_id=1, source_target_pairs={{0,8},{8,16},{16,24},{1,9},{9,17},{17,25},{2,10},{10,18},{18,26},{... | collective-permute-start | bytes 6152 | tf_op jit(solution)/shard_map/ppermute | solution.py:18
Sparse Core Ops, SparseCore 0:
  11.5 42.1 all-gather.6
  55.2 39.4 all-gather.8
  126.6 54.0 reduce-scatter.2
  221.0 30.3 all-gather.10
  252.8 29.8 all-gather.12
  286.2 6.3 reduce-scatter.4
where the time goes:
time: 313 us; the launch traced here: 312 us
  blocking collectives  165 us (53%)
  waiting for transfers between devices  70.9 us (23%)
  local copies, waits for them, and re-layouts  23.9 us (8%)
  matrix products  23.6 us (8%)
  between operations  13.8 us (4%)
  other arithmetic  12 us (4%)
    reduce_scatter x1, waiting for transfers between devices, shards(): lax.psum_scatter(project_in().astype(jnp.bfloat16), 'fs', scatter_dimensi...  36.4 us
    all_gather x1, waiting for transfers between devices, shards(): lax.all_gather(attn_out_weight, 'sp', axis=1, tiled=True)  26.6 us
    all_gather x1, blocking collectives, shards(): lax.all_gather(query_rope_weight, 'sp', axis=0, tiled=True)  22.8 us
    all_gather x1, blocking collectives, shards(): lax.all_gather(latent_weight, 'sp', axis=0, tiled=True)  17.8 us
    all_gather x1, blocking collectives, shards(): latent_piece = lax.all_gather(latent, 'sp', axis=0, tiled=True)  17.8 us
    all_gather x1, blocking collectives, shards(): lax.all_gather(conv_b_weight, 'sp', axis=0, tiled=True)  17.5 us
    all_gather x1, blocking collectives, shards(): lax.all_gather(conv_v_weight, 'sp', axis=0, tiled=True)  16.7 us
    all_gather x1, blocking collectives, shards(): lax.all_gather(conv_c_weight, 'sp', axis=0, tiled=True)  16.5 us
  transfers between devices with their start and end apart: 7, of which 3 were waited for; matrix products, arithmetic and copies ran while one was open for 8% of the time, Pallas kernels for 0%

commit v1 on v0

--- a/solution.py
+++ b/solution.py
@@ -157,8 +157,12 @@
         jnp.zeros((tok_rows, local_heads), jnp.float32),
         jnp.zeros((tok_rows, local_heads, KVL), jnp.float32),
     )
-    latent_piece = lax.all_gather(latent, "sp", axis=0, tiled=True)
-    rot_piece = lax.all_gather(key_rot, "sp", axis=0, tiled=True)
+    blocks_check = lambda own_rows, local_block: jnp.split(
+        lax.all_gather(jnp.concatenate([own_rows, local_block], axis=1), "sp", axis=0, tiled=True),
+        [own_rows.shape[1]],
+        axis=1,
+    )
+    latent_piece, rot_piece = blocks_check(latent, local_block=key_rot)
     piece_rows = latent_piece.shape[0]
     splits = max(1, piece_rows // 512)
     while piece_rows % splits:

time: 313 us -> 313 us (level)
  waiting for transfers between devices: 70.9 us -> 86.3 us
  blocking collectives: 165 us -> 153 us
  local copies, waits for them, and re-layouts: 23.9 us -> 20.7 us
    reduce_scatter x1, waiting for transfers between devices: 36.4 us -> 51.5 us  [shards(): lax.psum_scatter(project_in().astype(jnp.bfloat16), 'fs', scatter_dimensi...]
    all_gather x2 -> x1, blocking collectives: 31.9 us -> 19.9 us  [shards(): lax.all_gather(jnp.concatenate([own_rows, local_block], axis=1), 'sp', ax...]
where the time goes in v1:
time: 313 us; the launch traced here: 312 us
  blocking collectives  153 us (49%)
  waiting for transfers between devices  86.3 us (28%)
  matrix products  23.8 us (8%)
  local copies, waits for them, and re-layouts  20.7 us (7%)
  between operations  13.8 us (4%)
  other arithmetic  12.4 us (4%)
    reduce_scatter x1, waiting for transfers between devices, shards(): lax.psum_scatter(project_in().astype(jnp.bfloat16), 'fs', scatter_dimensi...  51.5 us
    all_gather x1, waiting for transfers between devices, shards(): lax.all_gather(attn_out_weight, 'sp', axis=1, tiled=True)  27 us
    all_gather x1, blocking collectives, shards(): lax.all_gather(query_rope_weight, 'sp', axis=0, tiled=True)  22.8 us
    all_gather x1, blocking collectives, shards(): lax.all_gather(jnp.concatenate([own_rows, local_block], axis=1), 'sp', ax...  19.9 us
    all_gather x1, blocking collectives, shards(): lax.all_gather(latent_weight, 'sp', axis=0, tiled=True)  17.8 us
    all_gather x1, blocking collectives, shards(): lax.all_gather(conv_b_weight, 'sp', axis=0, tiled=True)  17.5 us
    all_gather x1, blocking collectives, shards(): lax.all_gather(conv_v_weight, 'sp', axis=0, tiled=True)  16.7 us
    all_gather x1, blocking collectives, shards(): lax.all_gather(conv_c_weight, 'sp', axis=0, tiled=True)  16.5 us
  transfers between devices with their start and end apart: 7, of which 3 were waited for; matrix products, arithmetic and copies ran while one was open for 8% of the time, Pallas kernels for 0%

profile of v1, /device:TPU:0, one launch (start us, length us, event | category | flops | bytes accessed | tf_op | source)
XLA Modules:
  0.0 311.9 jit_solution(18355218734900224190)
XLA Ops:
  6.6 2.7 all-gather
  9.5 1.8 fusion.23
  11.4 0.7 all-gather.8.cloned.1.call-update
  12.2 17.5 %all_gather.41 = bf16[512,512]{1,0:T(8,128)(2,1)S(1)} all-gather(bf16[128,512]{1,0:T(8,128)(2,1)S(1)} %copy-done.8), channel_id=1, replica_groups=mesh['sp'=4,'fs'=4,'tp'=2] {'sp'}, dimensions={0}, use_global_device_ids=true | all-gather | bytes 655360 | tf_op jit(solution)/shard_map/all_gather | solution.py:78
  29.6 16.5 %all_gather.42 = bf16[512,512]{1,0:T(8,128)(2,1)} all-gather(bf16[128,512]{1,0:T(8,128)(2,1)S(1)} %copy-done.9), channel_id=1, replica_groups=mesh['sp'=4,'fs'=4,'tp'=2] {'sp'}, dimensions={0}, use_global_device_ids=true | all-gather | bytes 655360 | tf_op jit(solution)/shard_map/all_gather | solution.py:79
  46.1 16.7 %all_gather.43 = bf16[512,512]{1,0:T(8,128)(2,1)} all-gather(bf16[128,512]{1,0:T(8,128)(2,1)S(1)} %copy-done.10), channel_id=1, replica_groups=mesh['sp'=4,'fs'=4,'tp'=2] {'sp'}, dimensions={0}, use_global_device_ids=true | all-gather | bytes 655360 | tf_op jit(solution)/shard_map/all_gather | solution.py:80
  62.8 22.8 %all_gather.45 = bf16[512,512]{1,0:T(8,128)(2,1)S(1)} all-gather(bf16[128,512]{1,0:T(8,128)(2,1)S(1)} %copy-done.11), channel_id=1, replica_groups=mesh['sp'=4,'fs'=4,'tp'=2] {'sp'}, dimensions={0}, use_global_device_ids=true | all-gather | bytes 655360 | tf_op jit(solution)/shard_map/all_gather | solution.py:82
  85.6 17.8 %all_gather.46 = bf16[512,512]{1,0:T(8,128)(2,1)} all-gather(bf16[128,512]{1,0:T(8,128)(2,1)S(1)} %copy-done.12), channel_id=1, replica_groups=mesh['sp'=4,'fs'=4,'tp'=2] {'sp'}, dimensions={0}, use_global_device_ids=true | all-gather | bytes 655360 | tf_op jit(solution)/shard_map/all_gather | solution.py:83
  103.4 4.5 %copy.67 = bf16[640,2048]{0,1:T(8,128)(2,1)} copy(bf16[640,2048]{1,0:T(8,128)(2,1)} %all-gather.6.cloned.1.call-done) | data formatting | bytes 5242880 | tf_op jit(solution)/shard_map/all_gather | solution.py:73
  107.9 1.1 constant_dynamic-slice_fusion
  109.9 2.5 convolution_convert_fusion.5
  112.4 1.3 copy.71
  113.8 2.5 convolution_convert_fusion.4
  116.3 1.3 copy.72
  117.6 0.9 constant_dynamic-update-slice_fusion.2
  118.6 0.9 constant_dynamic-update-slice_fusion.1
  119.5 0.9 constant_dynamic-update-slice_fusion
  120.4 3.3 %fusion.16 = bf16[640,3584]{1,0:T(8,128)(2,1)} fusion(bf16[640,3584]{1,0:T(8,128)(2,1)} %constant_dynamic-update-slice_fusion, bf16[640,512]{0,1:T(8,128)(2,1)S(1)} %bitcast.100, bf16[512,1024]{1,0:T(8,128)(2,1)} %all-gather.8.cloned.1.call-done), kind=kOutput, calls=%fused_computation.37 | convolution fusion | flops 671744000 | bytes 3014656 | tf_op jit(solution)/shard_map/dot_general | solution.py:88
  123.7 1.4 fusion.20
  125.1 1.4 fusion.19
  126.7 1.9 broadcast_in_dim.56
  129.3 51.5 %reduce-scatter.3.cloned.1.call-done = bf16[160,3584]{1,0:T(8,128)(2,1)} async-done(((bf16[640,3584]{1,0:T(8,128)(2,1)}), bf16[160,3584]{1,0:T(8,128)(2,1)}) %reduce-scatter.3.cloned.1.call-update) | async-done | bytes 1146896 | tf_op jit(solution)/shard_map/reduce_scatter | solution.py:92
  180.8 1.0 fusion.33
  181.9 1.2 fusion.35
  183.2 19.9 %all_gather.49 = bf16[640,576]{1,0:T(8,128)(2,1)S(1)} all-gather(bf16[160,576]{1,0:T(8,128)(2,1)S(1)} %pad_maximum_fusion.1), channel_id=1, replica_groups=mesh['sp'=4,'fs'=4,'tp'=2] {'sp'}, dimensions={0}, use_global_device_ids=true | all-gather | bytes 921600 | tf_op jit(solution)/shard_map/all_gather | solution.py:161
  203.1 0.9 slice_convert_fusion
  204.5 0.9 pad_maximum_fusion
  205.4 1.5 fusion.17
  206.9 10.1 %conditional.1 = ((f32[160,8]{1,0:T(8,128)S(1)}, f32[160,8,512]{2,1,0:T(8,128)})) conditional(s32[]{:T(128)} %convert_element_type.79, (f32[160,8]{1,0:T(8,128)S(1)}, f32[160,8,512]{2,1,0:T(8,128)}) %tuple.31, (s32[160]{0:T(256)S(1)}, s32[160]{0:T(256)S(1)}, s32[]{:T(128)}, bf16[640,576]{1,0:T(8,128)(2,1)S(1)}, ...), branch_computations={%region_3.4_spmd, %region_4.7_spmd.clone} | conditional | flops 1792195712 | bytes 47736404 | solution.py:176
  207.3 1.2 copy.66
  208.4 1.5 fusion.11
  210.0 1.9 select_reduce_fusion
  211.9 1.1 fusion.1
  213.6 1.8 multiply_add_fusion
  215.4 1.6 copy-done.2
  217.0 2.1 divide_convert_fusion
  219.1 1.2 multiply_reduce_fusion
  220.3 1.0 copy_bitcast_fusion
  222.0 1.5 collective-permute-start
  223.5 14.3 %all_gather.48 = bf16[512,512]{1,0:T(8,128)(2,1)S(1)} all-gather(bf16[512,128]{1,0:T(8,128)(2,1)S(1)} %copy-done.13), channel_id=1, replica_groups=mesh['sp'=4,'fs'=4,'tp'=2] {'sp'}, dimensions={1}, use_global_device_ids=true | all-gather | bytes 655360 | tf_op jit(solution)/shard_map/all_gather | solution.py:210
  237.9 1.0 fusion.41
  239.0 13.8 %all_gather.47 = bf16[640,512]{1,0:T(8,128)(2,1)S(1)} all-gather(bf16[160,512]{1,0:T(8,128)(2,1)S(1)} %fusion.41), channel_id=1, replica_groups=mesh['sp'=4,'fs'=4,'tp'=2] {'fs'}, dimensions={0}, use_global_device_ids=true | all-gather | bytes 819200 | tf_op jit(solution)/shard_map/all_gather | solution.py:196
  253.3 2.5 copy.82
  255.8 27.0 %all-gather.12.cloned.1.call-done = bf16[1024,512]{1,0:T(8,128)(2,1)} async-done(((bf16[1024,128]{1,0:T(8,128)(2,1)}), bf16[1024,512]{1,0:T(8,128)(2,1)}) %all-gather.12.cloned.1.call-update) | async-done | bytes 1048592 | tf_op jit(solution)/shard_map/all_gather | solution.py:211
  282.8 3.3 %fusion.18 = bf16[640,512]{1,0:T(8,128)(2,1)} fusion(f32[640,512]{1,0:T(8,128)S(1)} %fusion.45, bf16[640,1024]{1,0:T(8,128)(2,1)} %bitcast.94, bf16[1024,512]{1,0:T(8,128)(2,1)} %all-gather.12.cloned.1.call-done), kind=kOutput, calls=%fused_computation.40 | convolution fusion | flops 671744000 | bytes 4325376 | tf_op jit(solution)/shard_map/dot_general | solution.py:216
  286.1 6.5 %reduce-scatter.5.cloned.1.call-done = bf16[320,512]{1,0:T(8,128)(2,1)} async-done(((bf16[640,512]{1,0:T(8,128)(2,1)}), bf16[320,512]{1,0:T(8,128)(2,1)}) %reduce-scatter.5.cloned.1.call-update) | async-done | bytes 327696 | tf_op jit(solution)/shard_map/reduce_scatter | solution.py:213
  292.6 11.0 %all_to_all.15 = bf16[4,80,512]{2,1,0:T(8,128)(2,1)S(1)} all-to-all(bf16[4,80,512]{2,1,0:T(8,128)(2,1)} %bitcast.103), channel_id=1, replica_groups=mesh['sp'=4,'fs'=4,'tp'=2] {'fs'}, dimensions={0} | all-to-all | bytes 655360 | tf_op jit(solution)/shard_map/all_to_all | solution.py:224
  304.1 1.0 broadcast_in_dim_reshape.4
  (77 shorter events, 5.2 us)
Async XLA Ops:
  6.5 198.9 %copy-start = (bf16[512,1024]{1,0:T(8,128)(2,1)S(1)}, bf16[512,1024]{1,0:T(8,128)(2,1)}, u32[]{:S(2)}) copy-start(bf16[512,1024]{1,0:T(8,128)(2,1)} %param.29) | copy-start | bytes 3145732
  6.5 5.6 %copy-start.8 = (bf16[128,512]{1,0:T(8,128)(2,1)S(1)}, bf16[128,512]{1,0:T(8,128)(2,1)}, u32[]{:S(2)}) copy-start(bf16[128,512]{1,0:T(8,128)(2,1)} %param.20) | copy-start | bytes 393220
  6.5 23.1 %copy-start.9 = (bf16[128,512]{1,0:T(8,128)(2,1)S(1)}, bf16[128,512]{1,0:T(8,128)(2,1)}, u32[]{:S(2)}) copy-start(bf16[128,512]{1,0:T(8,128)(2,1)} %param.21) | copy-start | bytes 393220
  6.5 39.6 %copy-start.10 = (bf16[128,512]{1,0:T(8,128)(2,1)S(1)}, bf16[128,512]{1,0:T(8,128)(2,1)}, u32[]{:S(2)}) copy-start(bf16[128,512]{1,0:T(8,128)(2,1)} %param.22) | copy-start | bytes 393220
  6.5 96.9 %all-gather.6.cloned.1.call-start = ((), (), s32[]{:S(2)}) async-start(), calls=%async_computation.3 | async-start | bytes 3276800 | tf_op jit(solution)/shard_map/all_gather | solution.py:73
  9.3 53.5 %copy-start.11 = (bf16[128,512]{1,0:T(8,128)(2,1)S(1)}, bf16[128,512]{1,0:T(8,128)(2,1)}, u32[]{:S(2)}) copy-start(bf16[128,512]{1,0:T(8,128)(2,1)} %param.25) | copy-start | bytes 393220
  9.3 76.3 %copy-start.12 = (bf16[128,512]{1,0:T(8,128)(2,1)S(1)}, bf16[128,512]{1,0:T(8,128)(2,1)}, u32[]{:S(2)}) copy-start(bf16[128,512]{1,0:T(8,128)(2,1)} %param.26) | copy-start | bytes 393220
  11.3 109.1 %all-gather.8.cloned.1.call-start = ((), (), s32[]{:S(2)}) async-start(), calls=%async_computation.4 | async-start | bytes 1310720 | tf_op jit(solution)/shard_map/all_gather | solution.py:81
  12.1 168.7 %reduce-scatter.3.cloned.1.call-start = ((), (), s32[]{:S(2)}) async-start(), calls=%async_computation.5 | async-start | bytes 5734400 | tf_op jit(solution)/shard_map/reduce_scatter | solution.py:92
  109.0 4.7 %copy-start.4 = (bf16[640,4,1,128]{0,3,2,1:T(8,128)(2,1)}, bf16[640,4,1,128]{0,3,2,1:T(8,128)(2,1)S(1)}, u32[]{:S(2)}) copy-start(bf16[640,4,1,128]{0,3,2,1:T(8,128)(2,1)S(1)} %constant_dynamic-slice_fusion) | copy-start | bytes 1966084
  118.6 1.8 copy-start.5
  120.4 4.7 %copy-start.6 = (bf16[512,512]{1,0:T(8,128)(2,1)S(1)}, bf16[512,512]{1,0:T(8,128)(2,1)}, u32[]{:S(2)}) copy-start(bf16[512,512]{1,0:T(8,128)(2,1)} %all_gather.46) | copy-start | bytes 1572868
  126.6 2.0 copy-start.3
  126.6 2.1 copy-start.7
  126.6 55.3 %copy-start.16 = (f32[512]{0:T(512)S(1)}, f32[512]{0:T(512)}, u32[]{:S(2)}) copy-start(f32[512]{0:T(512)} %param.28) | copy-start | bytes 6148
  126.6 126.7 %all-gather.10.cloned.1.call-start = ((), (), s32[]{:S(2)}) async-start(), calls=%async_computation.6 | async-start | bytes 1638400 | tf_op jit(solution)/shard_map/all_gather | solution.py:197
  211.8 1.7 copy-start.1
  215.4 1.6 copy-start.2
  217.0 2.1 copy-start.17
  219.1 1.2 copy-start.15
  219.1 2.8 copy-start.14
  219.1 4.4 %copy-start.13 = (bf16[512,128]{1,0:T(8,128)(2,1)S(1)}, bf16[512,128]{1,0:T(8,128)(2,1)}, u32[]{:S(2)}) copy-start(bf16[512,128]{1,0:T(8,128)(2,1)} %param.32) | copy-start | bytes 393220
  221.3 61.5 %all-gather.12.cloned.1.call-start = ((), (), s32[]{:S(2)}) async-start(), calls=%async_computation.7 | async-start | bytes 1310720 | tf_op jit(solution)/shard_map/all_gather | solution.py:211
  221.9 70.7 %reduce-scatter.5.cloned.1.call-start = ((), (), s32[]{:S(2)}) async-start(), calls=%async_computation.8 | async-start | bytes 983040 | tf_op jit(solution)/shard_map/reduce_scatter | solution.py:213
  222.0 15.9 %collective-permute-start = (bf16[2,512]{1,0:T(2,128)(2,1)S(1)}, bf16[2,512]{1,0:T(2,128)(2,1)S(1)}, u32[]{:S(2)}, u32[]{:S(2)}) collective-permute-start(bf16[2,512]{1,0:T(2,128)(2,1)S(1)} %slice.44), channel_id=1, source_target_pairs={{0,8},{8,16},{16,24},{1,9},{9,17},{17,25},{2,10},{10,18},{18,26},{... | collective-permute-start | bytes 6152 | tf_op jit(solution)/shard_map/ppermute | solution.py:18
Sparse Core Ops, SparseCore 0:
  11.5 42.1 all-gather.5
  55.2 39.4 all-gather.7
  126.7 54.0 reduce-scatter.2
  221.4 30.0 all-gather.9
  253.0 29.7 all-gather.11
  286.2 6.3 reduce-scatter.4
